TPU v7x, 128 devices: a whole 4x4x4 slice. The times are simulated.
128 devices in a mesh: fs: 16 (over z, y), tp: 8 (over x, core).
Axes of the slice: x: 4, y: 4, z: 4, core: 2. Of those that a mesh axis runs over, the one named last changes fastest.
Arguments:
- inputs: bfloat16 [49152, 2048], P('fs'), may hold values from -6 to 6
- cot_query: bfloat16 [49152, 2048], P('fs', 'tp'), may hold values from -0.0625 to 0.0625
- cot_value: bfloat16 [49152, 4096], P('fs', 'tp'), may hold values from -0.0625 to 0.0625
- proj_query: bfloat16 [2048, 256], replicated, may hold values from -0.375 to 0.375
- proj_value: bfloat16 [2048, 256], replicated, may hold values from -0.375 to 0.375
- w_query: float32 [2048, 2048], P('fs', 'tp'), may hold values from -6 to 6
- w_value: float32 [2048, 4096], P('fs', 'tp'), may hold values from -6 to 6
- m_query: float32 [256, 2048], P('fs', 'tp'), may hold values from -30 to 30
- m_value: float32 [256, 4096], P('fs', 'tp'), may hold values from -30 to 30
- v_query: float32 [256, 2048], P('fs', 'tp'), may hold values from 0.05 to 2
- v_value: float32 [256, 4096], P('fs', 'tp'), may hold values from 0.05 to 2
Outputs:
- new_query: float32 [2048, 2048], P('fs', 'tp')
- new_value: float32 [2048, 4096], P('fs', 'tp')
- copy_query: bfloat16 [2048, 2048], P(None, 'tp')
- copy_value: bfloat16 [2048, 4096], P(None, 'tp')
- first_query: float32 [256, 2048], P('fs', 'tp')
- first_value: float32 [256, 4096], P('fs', 'tp')
- second_query: float32 [256, 2048], P('fs', 'tp')
- second_value: float32 [256, 4096], P('fs', 'tp')
- step_query: float32 [2048, 2048], P('fs', 'tp')
- step_value: float32 [2048, 4096], P('fs', 'tp')
All inputs are finite; a program needn't handle non-finite values.
Results may differ from a plain program's by a relative error of at most 0.015.
Values may be sent and summed in bfloat16 or wider, within the bound.
No kernel may reach another device: no remote copies, remote signals or barrier semaphores. Data moves between devices by JAX's collectives and lax.ppermute only.
A program may use at most 128 MiB of HBM per device.

v0:
```python
import jax
import jax.numpy as jnp
from jax import lax
from jax.sharding import Mesh
from jax.sharding import PartitionSpec as P

RANK = 256
QK_W = 2048
V_W = 4096
FS = ("fs_0", "fs_1")
FS_TP = ("fs_0", "fs_1", "tp_0", "tp_1")
TP = ("tp_0", "tp_1")
beta_first = 0.9
beta_second = 0.95
adam_eps = 1e-08
norm_eps = 1e-06
step_rate = 0.05
decay_rate = 0.2


def cut_along(array, dim, length):
    lengths = array.shape
    pieces = array.reshape(*lengths[:dim], length, lengths[dim] // length, *lengths[dim + 1 :])
    return jnp.moveaxis(pieces, dim, 0)


def summed_on_arrival(array, axis, dim):
    length = lax.axis_size(axis)
    pieces = lax.all_to_all(cut_along(array, dim, length), axis, 0, 0, tiled=True)
    return jnp.sum(pieces, axis=0)


def by_axis(array, axes):
    for axis in axes:
        array = lax.psum(array, axis)
    return array


def sent_together(arrays, axis, dim, along):
    ends, at = ([], 0)
    for a in arrays[:-1]:
        at += a.shape[along]
        ends.append(at)
    both = jnp.concatenate(arrays, axis=along)
    return tuple(jnp.split(lax.all_gather(both, axis, axis=dim, tiled=True), ends, axis=along))


def moment_update(low, first, second):
    first_new = beta_first * first + (1.0 - beta_first) * low
    second_new = beta_second * second + (1.0 - beta_second) * low * low
    update = first_new / (jnp.sqrt(second_new) + adam_eps)
    return (first_new, second_new, update)


def lead_product(left, right):
    return lax.dot_general(
        left, right, (((0,), (0,)), ((), ())), preferred_element_type=jnp.float32
    )


def split_pair(values):
    upper = values.astype(jnp.bfloat16)
    lower = (values - upper.astype(jnp.float32)).astype(jnp.bfloat16)
    return (upper, lower)


def front_exact(factor, values):
    upper, lower = split_pair(values)
    return jnp.dot(factor, upper, preferred_element_type=jnp.float32) + jnp.dot(
        factor, lower, preferred_element_type=jnp.float32
    )


def on_device(
    inputs,
    cot_query,
    cot_value,
    proj_query,
    proj_value,
    w_query,
    w_value,
    m_query,
    m_value,
    v_query,
    v_value,
):
    rows = w_query.shape[0]
    width_query = cot_query.shape[1]
    offset = lax.axis_index(FS) * rows
    local_query = lax.dynamic_slice_in_dim(proj_query, offset, rows, 0)
    local_value = lax.dynamic_slice_in_dim(proj_value, offset, rows, 0)
    factor_query = proj_query
    factor_value = proj_value
    mixed_query = jnp.dot(inputs, factor_query, preferred_element_type=jnp.float32)
    mixed_value = jnp.dot(inputs, factor_value, preferred_element_type=jnp.float32)
    upper_query, lower_query = split_pair(mixed_query)
    upper_value, lower_value = split_pair(mixed_value)
    low = summed_on_arrival(
        jnp.concatenate(
            [
                lead_product(upper_query, cot_query) + lead_product(lower_query, cot_query),
                lead_product(upper_value, cot_value) + lead_product(lower_value, cot_value),
            ],
            axis=1,
        ),
        FS,
        0,
    )
    first_query, second_query, update_query = moment_update(low[:, :width_query], m_query, v_query)
    first_value, second_value, update_value = moment_update(low[:, width_query:], m_value, v_value)
    total = by_axis(
        jnp.sum(update_query * update_query) + jnp.sum(update_value * update_value), FS_TP
    )
    scale = lax.rsqrt(total / (RANK * (QK_W + V_W)) + norm_eps)
    pieces = sent_together((update_query, update_value), FS, 0, 1)
    factor_query = local_query
    factor_value = local_value
    back_query = front_exact(factor_query, pieces[0])
    back_value = front_exact(factor_value, pieces[1])
    step_query = scale * back_query + decay_rate * w_query
    step_value = scale * back_value + decay_rate * w_value
    new_query = w_query - step_rate * step_query
    new_value = w_value - step_rate * step_value
    copy_query, copy_value = sent_together(
        (new_query.astype(jnp.bfloat16), new_value.astype(jnp.bfloat16)), FS, 0, 1
    )
    return (
        new_query,
        new_value,
        copy_query,
        copy_value,
        first_query,
        first_value,
        second_query,
        second_value,
        step_query,
        step_value,
    )


def solution(mesh):
    finer = Mesh(mesh.devices.reshape(4, 4, 4, 2), ("fs_0", "fs_1", "tp_0", "tp_1"))
    placed = (
        P(FS, None),
        P(FS, TP),
        P(FS, TP),
        P(),
        P(),
        P(FS, TP),
        P(FS, TP),
        P(FS, TP),
        P(FS, TP),
        P(FS, TP),
        P(FS, TP),
    )
    return jax.shard_map(
        on_device,
        mesh=finer,
        in_specs=placed,
        out_specs=(
            P(FS, TP),
            P(FS, TP),
            P(None, TP),
            P(None, TP),
            P(FS, TP),
            P(FS, TP),
            P(FS, TP),
            P(FS, TP),
            P(FS, TP),
            P(FS, TP),
        ),
        check_vma=False,
    )
```

profile of v0, /device:TPU:1, one launch (start us, length us, event | category | flops | bytes accessed | tf_op | source)
XLA Modules:
  0.0 172.2 jit_solution(14548449293007263506)
XLA Ops:
  7.2 0.0 copy-start
  7.2 0.0 slice-start
  7.2 0.0 slice-start.1
  7.2 7.0 %fusion.31 = f32[3072,256]{1,0:T(8,128)S(1)} fusion(bf16[3072,2048]{1,0:T(8,128)(2,1)} %param.11, bf16[2048,256]{1,0:T(8,128)(2,1)} %param.15), kind=kOutput, calls=%fused_computation.50 | convolution fusion | flops 3221225472 | bytes 16777216 | tf_op jit(solution)/shard_map/dot_general | solution.py:95
  14.2 0.0 copy-done
  14.2 0.0 slice-start.2
  14.2 1.1 fusion.9
  15.3 0.0 copy-start.5
  15.3 1.9 %fusion.2 = f32[256,512]{1,0:T(8,128)} fusion(f32[256,512]{1,0:T(8,128)S(1)} %fusion.9, bf16[3072,512]{1,0:T(8,128)(2,1)S(1)} %copy-done, f32[3072,256]{1,0:T(8,128)S(1)} %fusion.31), kind=kOutput, calls=%fused_computation.4 | convolution fusion | flops 808583168 | bytes 7340032 | tf_op jit(solution)/shard_map/dot_general | solution.py:56
  17.1 0.0 slice-done
  17.1 0.0 slice-done.1
  17.1 0.0 slice-done.2
  17.1 0.0 copy-done.5
  17.1 0.0 copy-start.2
  17.2 3.6 %fusion.30 = f32[3072,256]{1,0:T(8,128)S(1)} fusion(bf16[3072,2048]{1,0:T(8,128)(2,1)S(1)} %bitcast.11, bf16[2048,256]{1,0:T(8,128)(2,1)S(1)} %copy-done.5), kind=kOutput, calls=%fused_computation.49 | convolution fusion | flops 3221225472 | bytes 16777216 | tf_op jit(solution)/shard_map/dot_general | solution.py:94
  20.7 0.0 copy-done.2
  20.8 0.7 fusion.12
  21.5 0.8 fusion.5
  22.3 0.0 copy-start.6
  22.3 0.0 copy-start.7
  22.3 0.0 copy-start.3
  22.3 0.0 copy-start.4
  22.3 0.8 copy.21
  23.2 2.0 %pad_maximum_fusion = f32[256,768]{1,0:T(8,128)} fusion(f32[256,512]{1,0:T(8,128)} %fusion.2, f32[256,256]{1,0:T(8,128)} %copy.21), kind=kLoop, calls=%fused_computation.12 | loop fusion | flops 196608 | bytes 1572864 | tf_op jit(solution)/shard_map/concatenate | solution.py:99
  25.2 8.6 %all-to-all-start = ((f32[16,16,768]{2,1,0:T(8,128)}), f32[16,16,768]{2,1,0:T(8,128)}, u32[]{:S(2)}, u32[]{:S(2)}) async-start(f32[16,16,768]{2,1,0:T(8,128)} %bitcast.9), calls=%async_computation | async-start | bytes 1572864 | tf_op jit(solution)/shard_map/all_to_all | solution.py:29
  33.9 0.0 all-gather.2.cloned.1.call-start
  33.9 13.2 %all-to-all-done = f32[16,16,768]{2,1,0:T(8,128)} async-done(((f32[16,16,768]{2,1,0:T(8,128)}), f32[16,16,768]{2,1,0:T(8,128)}, u32[]{:S(2)}, u32[]{:S(2)}) %all-to-all-start) | async-done | bytes 786464 | tf_op jit(solution)/shard_map/all_to_all | solution.py:29
  47.1 1.2 reduce_sum.27
  48.3 0.0 copy-done.6
  48.3 0.0 copy-done.7
  48.3 1.2 multiply_reduce_fusion.1
  49.6 0.0 copy-done.3
  49.6 0.0 copy-done.4
  49.6 1.2 multiply_reduce_fusion
  52.1 7.2 %psum.28 = f32[]{:T(128)} all-reduce(f32[]{:T(128)S(6)} %add.73), channel_id=1, replica_groups=mesh['fs_0'=4,'fs_1'=4,'tp_0'=4,'tp_1'=2] {'fs_0'}, use_global_device_ids=true, to_apply=%region_3.0 | all-reduce | flops 1 | bytes 8 | tf_op jit(solution)/shard_map/psum | solution.py:35
  59.3 7.4 %psum.29 = f32[]{:T(128)} all-reduce(f32[]{:T(128)} %psum.28), channel_id=1, replica_groups=mesh['fs_0'=4,'fs_1'=4,'tp_0'=4,'tp_1'=2] {'fs_1'}, use_global_device_ids=true, to_apply=%region_4.0 | all-reduce | flops 1 | bytes 8 | tf_op jit(solution)/shard_map/psum | solution.py:35
  66.7 9.1 %psum.30 = f32[]{:T(128)} all-reduce(f32[]{:T(128)} %psum.29), channel_id=1, replica_groups=mesh['fs_0'=4,'fs_1'=4,'tp_0'=4,'tp_1'=2] {'tp_0'}, use_global_device_ids=true, to_apply=%region_5.0 | all-reduce | flops 1 | bytes 8 | tf_op jit(solution)/shard_map/psum | solution.py:35
  75.8 17.5 %all_gather.6 = f32[256,768]{1,0:T(8,128)S(1)} all-gather(f32[16,768]{1,0:T(8,128)S(1)} %pad_maximum_fusion.2), channel_id=1, replica_groups=mesh['fs_0'=4,'fs_1'=4,'tp_0'=4,'tp_1'=2] {'fs_0','fs_1'}, dimensions={0}, use_global_device_ids=true | all-gather | bytes 835584 | tf_op jit(solution)/shard_map/all_gather | solution.py:45
  93.2 1.1 fusion.14
  94.3 1.0 fusion.18
  95.4 15.5 %psum.31 = f32[]{:T(128)} all-reduce(f32[]{:T(128)} %psum.30), channel_id=1, replica_groups=mesh['fs_0'=4,'fs_1'=4,'tp_0'=4,'tp_1'=2] {'tp_1'}, use_global_device_ids=true, to_apply=%region_6.0 | all-reduce | flops 1 | bytes 8 | tf_op jit(solution)/shard_map/psum | solution.py:35
  111.5 1.9 %fusion.26 = (bf16[128,256]{1,0:T(8,128)(2,1)S(1)}, f32[128,256]{1,0:T(8,128)}, f32[128,256]{1,0:T(8,128)}) fusion(f32[128,256]{1,0:T(8,128)} %param.16, f32[128,256]{1,0:T(8,128)S(1)} %fusion.18, f32[256,768]{1,0:T(8,128)} %copy-done.1, bf16[2048,256]{1,0:T(8,128)(2,1)} %param.14, s32[]{:T(128)S(6)} %select_n.4, f32[]{:T(128)S(6)} %rsqrt.3), kind=kOutput, calls=%fused_computation.47 | convolution fusion | flops 17268736 | bytes 917512 | tf_op jit(solution)/shard_map/dot_general | solution.py:69
  113.4 2.1 %fusion.27 = (bf16[128,512]{1,0:T(8,128)(2,1)S(1)}, f32[128,512]{1,0:T(8,128)}, f32[128,512]{1,0:T(8,128)}) fusion(f32[128,512]{1,0:T(8,128)} %param.17, f32[128,512]{1,0:T(8,128)S(1)} %fusion.14, f32[256,768]{1,0:T(8,128)} %copy-done.1, bf16[2048,256]{1,0:T(8,128)(2,1)} %param.15, s32[]{:T(128)S(6)} %select_n.4, f32[]{:T(128)S(6)} %rsqrt.3), kind=kOutput, calls=%fused_computation.48 | convolution fusion | flops 34537472 | bytes 1769480 | tf_op jit(solution)/shard_map/dot_general | solution.py:69
  115.5 0.7 pad_maximum_fusion.1
  116.2 0.0 all-gather.2.cloned.1.call-update
  116.3 43.8 %all-gather.2.cloned.1.call-done = bf16[2048,768]{1,0:T(8,128)(2,1)} async-done(((bf16[128,768]{1,0:T(8,128)(2,1)}), bf16[2048,768]{1,0:T(8,128)(2,1)}) %all-gather.2.cloned.1.call-update) | async-done | bytes 3145744 | tf_op jit(solution)/shard_map/all_gather | solution.py:45
  160.1 2.3 %split.18 = bf16[2048,256]{1,0:T(8,128)(2,1)} slice(bf16[2048,768]{1,0:T(8,128)(2,1)} %all-gather.2.cloned.1.call-done), slice={[0:2048], [0:256]} | slice | bytes 2097152 | tf_op jit(solution)/shard_map/split | solution.py:45
  162.3 3.0 %split.19 = bf16[2048,512]{1,0:T(8,128)(2,1)} slice(bf16[2048,768]{1,0:T(8,128)(2,1)} %all-gather.2.cloned.1.call-done), slice={[0:2048], [256:768]} | slice | bytes 4194304 | tf_op jit(solution)/shard_map/split | solution.py:45
  (4 shorter events, 0.0 us)
Async XLA Ops:
  7.2 7.0 %copy-start = (bf16[3072,512]{1,0:T(8,128)(2,1)S(1)}, bf16[3072,512]{1,0:T(8,128)(2,1)}, u32[]{:S(2)}) copy-start(bf16[3072,512]{1,0:T(8,128)(2,1)} %param.13) | copy-start | bytes 9437188
  7.2 9.9 %slice-start = ((s8[12582912]{0:T(1024)(128)(4,1)}), s8[4194304]{0:T(1024)(128)(4,1)S(1)}, s32[]{:S(2)}) async-start(s8[12582912]{0:T(1024)(128)(4,1)} %bitcast.10), calls=%async_computation.2 | async-start | bytes 8388608
  7.2 9.9 %slice-start.1 = ((s8[12582912]{0:T(1024)(128)(4,1)}), s8[4194304]{0:T(1024)(128)(4,1)S(1)}, s32[]{:S(2)}) async-start(s8[12582912]{0:T(1024)(128)(4,1)} %bitcast.10), calls=%async_computation.3 | async-start | bytes 8388608
  14.2 2.9 %slice-start.2 = ((s8[12582912]{0:T(1024)(128)(4,1)}), s8[4194304]{0:T(1024)(128)(4,1)S(1)}, s32[]{:S(2)}) async-start(s8[12582912]{0:T(1024)(128)(4,1)} %bitcast.10), calls=%async_computation.4 | async-start | bytes 8388608
  15.3 1.9 %copy-start.5 = (bf16[2048,256]{1,0:T(8,128)(2,1)S(1)}, bf16[2048,256]{1,0:T(8,128)(2,1)}, u32[]{:S(2)}) copy-start(bf16[2048,256]{1,0:T(8,128)(2,1)} %param.14) | copy-start | bytes 3145732
  17.1 3.6 %copy-start.2 = (bf16[3072,256]{1,0:T(8,128)(2,1)S(1)}, bf16[3072,256]{1,0:T(8,128)(2,1)}, u32[]{:S(2)}) copy-start(bf16[3072,256]{1,0:T(8,128)(2,1)} %param.12) | copy-start | bytes 4718596
  22.3 26.0 %copy-start.6 = (f32[16,256]{1,0:T(8,128)S(1)}, f32[16,256]{1,0:T(8,128)}, u32[]{:S(2)}) copy-start(f32[16,256]{1,0:T(8,128)} %param.20) | copy-start | bytes 49156
  22.3 26.0 %copy-start.7 = (f32[16,256]{1,0:T(8,128)S(1)}, f32[16,256]{1,0:T(8,128)}, u32[]{:S(2)}) copy-start(f32[16,256]{1,0:T(8,128)} %param.18) | copy-start | bytes 49156
  22.3 27.2 %copy-start.3 = (f32[16,512]{1,0:T(8,128)S(1)}, f32[16,512]{1,0:T(8,128)}, u32[]{:S(2)}) copy-start(f32[16,512]{1,0:T(8,128)} %param.21) | copy-start | bytes 98308
  22.3 27.2 %copy-start.4 = (f32[16,512]{1,0:T(8,128)S(1)}, f32[16,512]{1,0:T(8,128)}, u32[]{:S(2)}) copy-start(f32[16,512]{1,0:T(8,128)} %param.19) | copy-start | bytes 98308
  25.2 21.9 %all-to-all-start = ((f32[16,16,768]{2,1,0:T(8,128)}), f32[16,16,768]{2,1,0:T(8,128)}, u32[]{:S(2)}, u32[]{:S(2)}) async-start(f32[16,16,768]{2,1,0:T(8,128)} %bitcast.9), calls=%async_computation | async-start | bytes 1572864 | tf_op jit(solution)/shard_map/all_to_all | solution.py:29
  33.9 126.2 %all-gather.2.cloned.1.call-start = ((), (), s32[]{:S(2)}) async-start(), calls=%async_computation.1 | async-start | bytes 3342336 | tf_op jit(solution)/shard_map/all_gather | solution.py:45
  93.2 1.1 copy-start.1
Sparse Core Ops, SparseCore 0:
  116.4 43.6 all-gather.1
where the time goes:
time: 173 us; the launch traced here: 172 us
  waiting for transfers between devices  57.1 us (33%)
  blocking collectives  56.6 us (33%)
  matrix products  21.1 us (12%)
  between operations  16.2 us (9%)
  starting transfers between devices  8.67 us (5%)
  other arithmetic  6.36 us (4%)
  local copies, waits for them, and re-layouts  6.21 us (4%)
    all_gather x1, waiting for transfers between devices, sent_together(): lax.all_gather(both, axis, axis=dim, tiled=True)  43.8 us
    psum x4, blocking collectives, by_axis(): array = lax.psum(array, axis)  39.1 us
    all_gather x1, blocking collectives, sent_together(): lax.all_gather(both, axis, axis=dim, tiled=True)  17.5 us
    all_to_all x1, waiting for transfers between devices, summed_on_arrival(): lax.all_to_all(cut_along(array, dim, length), axis, 0, 0, tiled=True)  13.2 us
    all_to_all x1, starting transfers between devices, summed_on_arrival(): lax.all_to_all(cut_along(array, dim, length), axis, 0, 0, tiled=True)  8.63 us
    dot_general x1, matrix products, on_device(): jnp.dot(inputs, factor_value, preferred_element_type=jnp.float32)  6.95 us
    split x2, local copies, waits for them, and re-layouts, sent_together(): jnp.split(lax.all_gather(both, axis, axis=dim, tiled=True), ends, axis=al...  5.3 us
    dot_general x4, matrix products, lead_product(): lax.dot_general(left, right, (((0,), (0,)), ((), ())), preferred_element_...  4.44 us
  transfers between devices with their start and end apart: 2, of which 2 were waited for; matrix products, arithmetic and copies ran while one was open for 0% of the time, Pallas kernels for 0%

commit v1 on v0

--- a/solution.py
+++ b/solution.py
@@ -32,7 +32,7 @@
 
 def by_axis(array, axes):
     for axis in axes:
-        array = lax.psum(array, axis)
+        array = jnp.sum(lax.all_gather(array, axis), axis=0)
     return array
 
 

time: 173 us -> 181 us (1.046)
  local copies, waits for them, and re-layouts: 6.21 us -> 13.5 us
  other arithmetic: 6.36 us -> 8.78 us
    psum x4 -> x0, blocking collectives: 39.1 us -> none  [by_axis(): array = lax.psum(array, axis)]
    unnamed x0 -> x4, blocking collectives: none -> 36.3 us
    unnamed x22 -> x40, local copies, waits for them, and re-layouts: 0.07 us -> 7.4 us
    reduce_sum x0 -> x4, other arithmetic: none -> 2.41 us  [by_axis(): array = jnp.sum(lax.all_gather(array, axis), axis=0)]
    all_gather x1, blocking collectives: 17.5 us -> 19.8 us  [sent_together(): lax.all_gather(both, axis, axis=dim, tiled=True)]
  transfers between devices with their start and end apart: 2 -> 2, of which waited for: 2 -> 2; matrix products, arithmetic and copies ran while one was open for 0% -> 1% of each run, Pallas kernels for 0% -> 0%
where the time goes in v1:
time: 181 us
  blocking collectives  56.1 us (31%)
  waiting for transfers between devices  56 us (31%)
  matrix products  21.4 us (12%)
  between operations  16.3 us (9%)
  local copies, waits for them, and re-layouts  13.5 us (7%)
  other arithmetic  8.78 us (5%)
  starting transfers between devices  8.67 us (5%)
    all_gather x1, waiting for transfers between devices, sent_together(): lax.all_gather(both, axis, axis=dim, tiled=True)  43.9 us
    unnamed x4, blocking collectives  36.3 us
    all_gather x1, blocking collectives, sent_together(): lax.all_gather(both, axis, axis=dim, tiled=True)  19.8 us
    all_to_all x1, waiting for transfers between devices, summed_on_arrival(): lax.all_to_all(cut_along(array, dim, length), axis, 0, 0, tiled=True)  12 us
    all_to_all x1, starting transfers between devices, summed_on_arrival(): lax.all_to_all(cut_along(array, dim, length), axis, 0, 0, tiled=True)  8.63 us
    unnamed x40, local copies, waits for them, and re-layouts  7.4 us
    dot_general x1, matrix products, on_device(): jnp.dot(inputs, factor_value, preferred_element_type=jnp.float32)  6.95 us
    split x2, local copies, waits for them, and re-layouts, sent_together(): jnp.split(lax.all_gather(both, axis, axis=dim, tiled=True), ends, axis=al...  5.3 us
  transfers between devices with their start and end apart: 2, of which 2 were waited for; matrix products, arithmetic and copies ran while one was open for 1% of the time, Pallas kernels for 0%

profile of v1, /device:TPU:1, one launch (start us, length us, event | category | flops | bytes accessed | tf_op | source)
XLA Modules:
  0.0 180.8 jit_solution(10098592090564759640)
XLA Ops:
  7.2 0.0 copy-start
  7.2 0.0 slice-start
  7.2 7.0 %fusion.31 = f32[3072,256]{1,0:T(8,128)S(1)} fusion(bf16[3072,2048]{1,0:T(8,128)(2,1)} %param.11, bf16[2048,256]{1,0:T(8,128)(2,1)} %param.15), kind=kOutput, calls=%fused_computation.50 | convolution fusion | flops 3221225472 | bytes 16777216 | tf_op jit(solution)/shard_map/dot_general | solution.py:95
  14.2 0.0 slice-start.2
  14.2 1.1 fusion.9
  15.3 1.9 %fusion.2 = f32[256,512]{1,0:T(8,128)} fusion(f32[256,512]{1,0:T(8,128)S(1)} %fusion.9, bf16[3072,512]{1,0:T(8,128)(2,1)S(1)} %copy-done, f32[3072,256]{1,0:T(8,128)S(1)} %fusion.31), kind=kOutput, calls=%fused_computation.4 | convolution fusion | flops 808583168 | bytes 7340032 | tf_op jit(solution)/shard_map/dot_general | solution.py:56
  17.2 3.6 %fusion.30 = f32[3072,256]{1,0:T(8,128)S(1)} fusion(bf16[3072,2048]{1,0:T(8,128)(2,1)S(1)} %bitcast.19, bf16[2048,256]{1,0:T(8,128)(2,1)S(1)} %copy-done.4), kind=kOutput, calls=%fused_computation.49 | convolution fusion | flops 3221225472 | bytes 16777216 | tf_op jit(solution)/shard_map/dot_general | solution.py:94
  20.8 0.7 fusion.12
  21.5 0.8 fusion.5
  22.3 0.0 copy-start.10
  22.3 0.0 copy-start.9
  22.3 0.0 copy-start.5
  22.4 0.0 copy-start.8
  22.4 0.0 copy-start.7
  22.4 0.8 copy.21
  23.2 2.0 %pad_maximum_fusion = f32[256,768]{1,0:T(8,128)} fusion(f32[256,512]{1,0:T(8,128)} %fusion.2, f32[256,256]{1,0:T(8,128)} %copy.21), kind=kLoop, calls=%fused_computation.12 | loop fusion | flops 196608 | bytes 1572864 | tf_op jit(solution)/shard_map/concatenate | solution.py:99
  25.3 8.6 %all-to-all-start = ((f32[16,16,768]{2,1,0:T(8,128)}), f32[16,16,768]{2,1,0:T(8,128)}, u32[]{:S(2)}, u32[]{:S(2)}) async-start(f32[16,16,768]{2,1,0:T(8,128)} %bitcast.17), calls=%async_computation | async-start | bytes 1572864 | tf_op jit(solution)/shard_map/all_to_all | solution.py:29
  33.9 0.0 all-gather.2.cloned.1.call-start
  34.0 0.6 dynamic-slice.3
  34.6 0.6 dynamic-slice
  35.2 12.0 %all-to-all-done = f32[16,16,768]{2,1,0:T(8,128)} async-done(((f32[16,16,768]{2,1,0:T(8,128)}), f32[16,16,768]{2,1,0:T(8,128)}, u32[]{:S(2)}, u32[]{:S(2)}) %all-to-all-start) | async-done | bytes 786464 | tf_op jit(solution)/shard_map/all_to_all | solution.py:29
  47.2 1.2 reduce_sum.63
  48.4 1.2 multiply_reduce_fusion.1
  49.6 1.2 multiply_reduce_fusion
  52.2 0.8 dynamic-update-slice
  52.9 0.6 dynamic-slice.1
  53.5 6.7 %all-reduce = f32[4]{0:T(128)S(1)} all-reduce(f32[4]{0:T(128)S(1)} %dynamic-update-slice), channel_id=1, replica_groups=mesh['fs_0'=4,'fs_1'=4,'tp_0'=4,'tp_1'=2] {'fs_0'}, use_global_device_ids=true, to_apply=%add | all-reduce | flops 4 | bytes 32
  60.2 0.6 reduce_sum.66
  60.8 1.4 dynamic-update-slice.1
  62.2 0.6 dynamic-slice.2
  62.8 6.7 %all-reduce.1 = f32[4]{0:T(128)S(1)} all-reduce(f32[4]{0:T(128)S(1)} %dynamic-update-slice.1), channel_id=1, replica_groups=mesh['fs_0'=4,'fs_1'=4,'tp_0'=4,'tp_1'=2] {'fs_1'}, use_global_device_ids=true, to_apply=%add.1 | all-reduce | flops 4 | bytes 32
  69.5 0.6 reduce_sum.67
  70.1 1.4 dynamic-update-slice.2
  71.5 8.5 %all-reduce.2 = f32[4]{0:T(128)S(1)} all-reduce(f32[4]{0:T(128)S(1)} %dynamic-update-slice.2), channel_id=1, replica_groups=mesh['fs_0'=4,'fs_1'=4,'tp_0'=4,'tp_1'=2] {'tp_0'}, use_global_device_ids=true, to_apply=%add.2 | all-reduce | flops 4 | bytes 32
  80.0 19.8 %all_gather.38 = f32[256,768]{1,0:T(8,128)} all-gather(f32[16,768]{1,0:T(8,128)S(1)} %pad_maximum_fusion.2), channel_id=1, replica_groups=mesh['fs_0'=4,'fs_1'=4,'tp_0'=4,'tp_1'=2] {'fs_0','fs_1'}, dimensions={0}, use_global_device_ids=true | all-gather | bytes 835584 | tf_op jit(solution)/shard_map/all_gather | solution.py:45
  99.8 0.6 reduce_sum.68
  100.4 1.3 fusion.14
  101.6 1.4 dynamic-update-slice.3
  103.0 1.1 fusion.18
  104.2 14.5 %all-reduce.3 = f32[2]{0:T(128)S(1)} all-reduce(f32[2]{0:T(128)S(1)} %dynamic-update-slice.3), channel_id=1, replica_groups=mesh['fs_0'=4,'fs_1'=4,'tp_0'=4,'tp_1'=2] {'tp_1'}, use_global_device_ids=true, to_apply=%add.3 | all-reduce | flops 2 | bytes 16
  118.7 0.6 reduce_sum.69
  120.0 1.9 %fusion.26 = (bf16[128,256]{1,0:T(8,128)(2,1)S(1)}, f32[128,256]{1,0:T(8,128)}, f32[128,256]{1,0:T(8,128)}) fusion(f32[128,256]{1,0:T(8,128)} %param.16, f32[128,256]{1,0:T(8,128)S(1)} %fusion.18, f32[256,768]{1,0:T(8,128)} %all_gather.38, bf16[2048,256]{1,0:T(8,128)(2,1)} %param.14, s32[]{:T(128)S(6)} %select_n.4, f32[]{:T(128)S(6)} %rsqrt.3), kind=kOutput, calls=%fused_computation.47 | convolution fusion | flops 17268736 | bytes 917512 | tf_op jit(solution)/shard_map/dot_general | solution.py:69
  121.9 2.1 %fusion.27 = (bf16[128,512]{1,0:T(8,128)(2,1)S(1)}, f32[128,512]{1,0:T(8,128)}, f32[128,512]{1,0:T(8,128)}) fusion(f32[128,512]{1,0:T(8,128)} %param.17, f32[128,512]{1,0:T(8,128)S(1)} %fusion.14, f32[256,768]{1,0:T(8,128)} %all_gather.38, bf16[2048,256]{1,0:T(8,128)(2,1)} %param.15, s32[]{:T(128)S(6)} %select_n.4, f32[]{:T(128)S(6)} %rsqrt.3), kind=kOutput, calls=%fused_computation.48 | convolution fusion | flops 34537472 | bytes 1769480 | tf_op jit(solution)/shard_map/dot_general | solution.py:69
  124.0 0.7 pad_maximum_fusion.1
  124.7 0.0 all-gather.2.cloned.1.call-update
  124.7 43.9 %all-gather.2.cloned.1.call-done = bf16[2048,768]{1,0:T(8,128)(2,1)} async-done(((bf16[128,768]{1,0:T(8,128)(2,1)}), bf16[2048,768]{1,0:T(8,128)(2,1)}) %all-gather.2.cloned.1.call-update) | async-done | bytes 3145744 | tf_op jit(solution)/shard_map/all_gather | solution.py:45
  168.6 2.3 %split.18 = bf16[2048,256]{1,0:T(8,128)(2,1)} slice(bf16[2048,768]{1,0:T(8,128)(2,1)} %all-gather.2.cloned.1.call-done), slice={[0:2048], [0:256]} | slice | bytes 2097152 | tf_op jit(solution)/shard_map/split | solution.py:45
  170.9 3.0 %split.19 = bf16[2048,512]{1,0:T(8,128)(2,1)} slice(bf16[2048,768]{1,0:T(8,128)(2,1)} %all-gather.2.cloned.1.call-done), slice={[0:2048], [256:768]} | slice | bytes 4194304 | tf_op jit(solution)/shard_map/split | solution.py:45
  (26 shorter events, 0.1 us)
Async XLA Ops:
  7.2 7.0 %copy-start = (bf16[3072,512]{1,0:T(8,128)(2,1)S(1)}, bf16[3072,512]{1,0:T(8,128)(2,1)}, u32[]{:S(2)}) copy-start(bf16[3072,512]{1,0:T(8,128)(2,1)} %param.13) | copy-start | bytes 9437188
  7.2 9.9 %slice-start = ((s8[12582912]{0:T(1024)(128)(4,1)}), s8[4194304]{0:T(1024)(128)(4,1)S(1)}, s32[]{:S(2)}) async-start(s8[12582912]{0:T(1024)(128)(4,1)} %bitcast.18), calls=%async_computation.2 | async-start | bytes 8388608
  7.2 9.9 %slice-start.1 = ((s8[12582912]{0:T(1024)(128)(4,1)}), s8[4194304]{0:T(1024)(128)(4,1)S(1)}, s32[]{:S(2)}) async-start(s8[12582912]{0:T(1024)(128)(4,1)} %bitcast.18), calls=%async_computation.3 | async-start | bytes 8388608
  14.2 2.9 %slice-start.2 = ((s8[12582912]{0:T(1024)(128)(4,1)}), s8[4194304]{0:T(1024)(128)(4,1)S(1)}, s32[]{:S(2)}) async-start(s8[12582912]{0:T(1024)(128)(4,1)} %bitcast.18), calls=%async_computation.4 | async-start | bytes 8388608
  15.3 1.9 %copy-start.4 = (bf16[2048,256]{1,0:T(8,128)(2,1)S(1)}, bf16[2048,256]{1,0:T(8,128)(2,1)}, u32[]{:S(2)}) copy-start(bf16[2048,256]{1,0:T(8,128)(2,1)} %param.14) | copy-start | bytes 3145732
  17.1 3.6 %copy-start.1 = (bf16[3072,256]{1,0:T(8,128)(2,1)S(1)}, bf16[3072,256]{1,0:T(8,128)(2,1)}, u32[]{:S(2)}) copy-start(bf16[3072,256]{1,0:T(8,128)(2,1)} %param.12) | copy-start | bytes 4718596
  22.3 11.7 %copy-start.10 = (u32[128]{0:T(128)S(1)}, u32[128]{0:T(128)}, u32[]{:S(2)}) copy-start(u32[128]{0:T(128)} %constant.61) | copy-start | bytes 1540
  22.3 12.3 %copy-start.9 = (u32[128]{0:T(128)S(1)}, u32[128]{0:T(128)}, u32[]{:S(2)}) copy-start(u32[128]{0:T(128)} %constant.13) | copy-start | bytes 1540
  22.3 26.1 %copy-start.5 = (f32[16,256]{1,0:T(8,128)S(1)}, f32[16,256]{1,0:T(8,128)}, u32[]{:S(2)}) copy-start(f32[16,256]{1,0:T(8,128)} %param.20) | copy-start | bytes 49156
  22.3 26.1 %copy-start.6 = (f32[16,256]{1,0:T(8,128)S(1)}, f32[16,256]{1,0:T(8,128)}, u32[]{:S(2)}) copy-start(f32[16,256]{1,0:T(8,128)} %param.18) | copy-start | bytes 49156
  22.4 27.3 %copy-start.2 = (f32[16,512]{1,0:T(8,128)S(1)}, f32[16,512]{1,0:T(8,128)}, u32[]{:S(2)}) copy-start(f32[16,512]{1,0:T(8,128)} %param.21) | copy-start | bytes 98308
  22.4 27.3 %copy-start.3 = (f32[16,512]{1,0:T(8,128)S(1)}, f32[16,512]{1,0:T(8,128)}, u32[]{:S(2)}) copy-start(f32[16,512]{1,0:T(8,128)} %param.19) | copy-start | bytes 98308
  22.4 30.6 %copy-start.8 = (u32[128]{0:T(128)S(1)}, u32[128]{0:T(128)}, u32[]{:S(2)}) copy-start(u32[128]{0:T(128)} %constant.51) | copy-start | bytes 1540
  22.4 39.8 %copy-start.7 = (u32[128]{0:T(128)S(1)}, u32[128]{0:T(128)}, u32[]{:S(2)}) copy-start(u32[128]{0:T(128)} %constant.56) | copy-start | bytes 1540
  25.3 21.9 %all-to-all-start = ((f32[16,16,768]{2,1,0:T(8,128)}), f32[16,16,768]{2,1,0:T(8,128)}, u32[]{:S(2)}, u32[]{:S(2)}) async-start(f32[16,16,768]{2,1,0:T(8,128)} %bitcast.17), calls=%async_computation | async-start | bytes 1572864 | tf_op jit(solution)/shard_map/all_to_all | solution.py:29
  33.9 134.7 %all-gather.2.cloned.1.call-start = ((), (), s32[]{:S(2)}) async-start(), calls=%async_computation.1 | async-start | bytes 3342336 | tf_op jit(solution)/shard_map/all_gather | solution.py:45
Sparse Core Ops, SparseCore 0:
  124.8 43.7 all-gather.1
